TPU v7x, 128 devices: a whole 4x4x4 slice. The times are simulated.
128 devices in a mesh: ep: 16 (over z, x), tp: 8 (over y, core).
Axes of the slice: x: 4, y: 4, z: 4, core: 2. Of those that a mesh axis runs over, the one named last changes fastest.
Arguments:
- out_gate: bfloat16 [32768, 1024], P('ep', 'tp'), may hold values from -6 to 6
- in_gate: bfloat16 [32768, 1024], P('ep', 'tp'), may hold values from -6 to 6
- conv_input: bfloat16 [32768, 1024], P('ep', 'tp'), may hold values from -6 to 6
- conv_taps: float32 [3, 1024], P(None, 'tp'), may hold values from -4 to 4
- group_gain: float32 [1024], P('tp'), may hold values from 0.1 to 1.9
- mix_out_w: bfloat16 [1024, 2048], replicated, may hold values from -0.1875 to 0.1875
- moe_in: bfloat16 [32768, 2048], P(('ep', 'tp')), may hold values from -6 to 6
- moe_gain: float32 [2048], replicated, may hold values from 0.1 to 1.9
- route_ids: int32 [32768, 2], P(('ep', 'tp')), may hold values from 0 to 127, as said below
- route_weight: float32 [32768, 2], P(('ep', 'tp')), may hold values from 0.1 to 1
- gate_w: bfloat16 [128, 2048, 1024], P(('ep', 'tp')), may hold values from -0.125 to 0.125
- up_w: bfloat16 [128, 2048, 1024], P(('ep', 'tp')), may hold values from -0.125 to 0.125
- down_w: bfloat16 [128, 1024, 2048], P(('ep', 'tp')), may hold values from -0.1875 to 0.1875
Outputs:
- mixed: bfloat16 [32768, 2048], P(('ep', 'tp'))
- moe_out: bfloat16 [32768, 2048], P(('ep', 'tp'))
Inputs may be any that keep to these rules, and one draw needn't show every extreme that they name: `route_ids`: the two numbers of a row are different experts of one group: group g holds experts g * 8 to g * 8 + 7. The rows of one device (aligned blocks of 256 rows) name each group in exactly 16 rows and each expert in exactly 4 rows.
All inputs are finite; a program needn't handle non-finite values.
Results may differ from a plain program's by a relative error of at most 0.0071.
Values may be sent and summed in bfloat16 or wider, within the bound.
A program may use at most 128 MiB of HBM per device.

v0:
```python
import jax
import jax.numpy as jnp
from jax import lax
from jax.sharding import PartitionSpec as P

GROUP_CH = 64


def shifted(value, axis, by):
    count = lax.axis_size(axis)
    pairs = [(i, i + by) for i in range(count) if 0 <= i + by < count]
    return lax.ppermute(value, axis, pairs)


def expert_rows(inputs, w_gate, w_up, w_down):
    gate_part = jnp.dot(inputs, w_gate, preferred_element_type=jnp.float32)
    up_part = jnp.dot(inputs, w_up, preferred_element_type=jnp.float32)
    hidden = (jax.nn.silu(gate_part) * up_part).astype(jnp.bfloat16)
    return jnp.dot(hidden, w_down, preferred_element_type=jnp.float32).astype(jnp.bfloat16)


def place_ranks(labels_in, bins, per_bin):
    hits = (labels_in[:, None] == jnp.arange(bins, dtype=jnp.int32)[None, :]).astype(jnp.int32)
    before = jnp.cumsum(hits, axis=0) - hits
    return labels_in * per_bin + jnp.sum(before * hits, axis=1)


def shards(
    out_gate,
    in_gate,
    conv_input,
    conv_taps,
    group_gain,
    mix_out_w,
    moe_in,
    moe_gain,
    route_ids,
    route_weight,
    gate_w,
    up_w,
    down_w,
):
    rows_ep, channels = in_gate.shape
    member_count = lax.axis_size("tp")
    group_count = lax.axis_size("ep")
    reach = conv_taps.shape[0] - 1
    edge_rows = jnp.stack([in_gate[rows_ep - reach :], conv_input[rows_ep - reach :]])
    earlier = shifted(edge_rows, "ep", 1)
    product = in_gate.astype(jnp.float32) * conv_input.astype(jnp.float32)
    before_rows = earlier[0].astype(jnp.float32) * earlier[1].astype(jnp.float32)
    padded = jnp.concatenate([before_rows, product], axis=0)
    convolved = jnp.zeros_like(product)
    for tap in range(reach + 1):
        convolved = convolved + conv_taps[tap] * padded[tap : tap + rows_ep]
    gated = out_gate.astype(jnp.float32) * convolved
    grouped = gated.reshape(rows_ep, channels // GROUP_CH, GROUP_CH)
    inv_rms = lax.rsqrt(jnp.mean(grouped * grouped, axis=-1, keepdims=True) + 1e-06)
    normed = ((grouped * inv_rms).reshape(rows_ep, channels) * group_gain).astype(jnp.bfloat16)
    blocks = normed.reshape(member_count, rows_ep // member_count, channels)
    portion = lax.all_to_all(blocks, "tp", split_axis=0, concat_axis=2, tiled=True)
    flat_rows = portion.reshape(-1, portion.shape[2])
    projected = jnp.dot(flat_rows, mix_out_w, preferred_element_type=jnp.float32).astype(
        jnp.bfloat16
    )
    mixed = projected.reshape(portion.shape[0], portion.shape[1], -1)
    mixed = mixed.reshape(-1, mixed.shape[2])
    tok_count, width = moe_in.shape
    wide_in = moe_in.astype(jnp.float32)
    rms_scale = lax.rsqrt(jnp.mean(wide_in * wide_in, axis=-1, keepdims=True) + 1e-06)
    expert_in = (wide_in * rms_scale * moe_gain).astype(jnp.bfloat16)
    w_gate = gate_w[0]
    w_up = up_w[0]
    w_down = down_w[0]
    expert_count = group_count * member_count
    slot_count = 2 * tok_count // expert_count
    flat_ids = route_ids.reshape(-1)
    target = place_ranks(flat_ids, expert_count, slot_count)
    owners = jnp.arange(2 * tok_count, dtype=jnp.int32) // 2
    sources = jnp.zeros((expert_count * slot_count,), jnp.int32).at[target].set(owners)
    outgoing = expert_in[sources].reshape(expert_count, slot_count, width)
    portion = lax.all_to_all(outgoing, ("ep", "tp"), split_axis=0, concat_axis=0, tiled=True)
    sources, amount, _ = portion.shape
    returned = lax.all_to_all(
        expert_rows(portion.reshape(-1, width), w_gate, w_up, w_down).reshape(
            sources, amount, width
        ),
        ("ep", "tp"),
        split_axis=0,
        concat_axis=0,
        tiled=True,
    )
    results = returned.reshape(-1, width)[target].reshape(tok_count, 2, width)
    first_out = results[:, 0].astype(jnp.float32)
    second = results[:, 1].astype(jnp.float32)
    moe_out = (first_out * route_weight[:, 0:1] + second * route_weight[:, 1:2]).astype(
        jnp.bfloat16
    )
    return (mixed, moe_out)


def solution(mesh):
    in_specs = (
        P("ep", "tp"),
        P("ep", "tp"),
        P("ep", "tp"),
        P(None, "tp"),
        P("tp"),
        P(),
        P(("ep", "tp"), None),
        P(),
        P(("ep", "tp"), None),
        P(("ep", "tp"), None),
        P(("ep", "tp"), None, None),
        P(("ep", "tp"), None, None),
        P(("ep", "tp"), None, None),
    )
    out_specs = (P(("ep", "tp"), None), P(("ep", "tp"), None))
    return jax.shard_map(shards, mesh=mesh, in_specs=in_specs, out_specs=out_specs, check_vma=False)
```

profile of v0, /device:TPU:1, one launch (start us, length us, event | category | flops | bytes accessed | tf_op | source)
XLA Modules:
  0.0 133.1 jit_solution(3074338711786757007)
XLA Ops:
  0.6 0.0 copy-start
  0.6 0.0 copy-start.4
  0.6 0.9 copy.36
  1.6 0.1 eq.29
  1.7 0.1 eq.25
  1.8 0.7 broadcast_multiply_fusion
  2.5 0.1 copy.38
  2.6 0.2 fusion.28
  3.0 0.1 copy.35
  3.1 0.1 mul.159
  3.3 0.2 fusion.27
  3.5 2.4 %scatter_custom_fusion = s32[512]{0:T(512)S(1)} fusion(s32[512]{0:T(512)S(1)} %bitcast.81, s32[512]{0:T(512)S(1)} %add_select_fusion, s32[]{:T(128)} %constant.35.clone.1), kind=kCustom, calls=%fused_computation.63 | custom fusion | bytes 2052 | tf_op jit(solution)/shard_map/scatter | solution.py:79
  6.0 0.0 copy-done
  6.0 0.3 fusion.9
  6.3 0.0 copy-done.4
  6.3 0.3 fusion.11
  6.6 2.5 %gather_fusion = bf16[512,2048]{1,0:T(8,128)(2,1)S(1)} fusion(bf16[256,2048]{1,0:T(8,128)(2,1)S(1)} %fusion.11, s32[1024]{0:T(1024)S(1)} %pad_clamp_fusion.1), kind=kCustom, calls=%fused_computation | custom fusion | bytes 4196352 | tf_op jit(solution)/shard_map/gather | solution.py:80
  9.1 2.2 %reshape.104 = bf16[128,4,2048]{2,1,0:T(4,128)(2,1)} reshape(bf16[512,2048]{1,0:T(8,128)(2,1)S(1)} %gather_fusion) | data formatting | bytes 4194304 | tf_op jit(solution)/shard_map/reshape | solution.py:80
  11.3 11.5 %all-to-all-start.1 = ((bf16[128,4,2048]{2,1,0:T(4,128)(2,1)}), bf16[128,4,2048]{2,1,0:T(4,128)(2,1)S(1)}, u32[]{:S(2)}, u32[]{:S(2)}) async-start(bf16[128,4,2048]{2,1,0:T(4,128)(2,1)} %reshape.104), calls=%async_computation.1 | async-start | bytes 4194304 | tf_op jit(solution)/shard_map/all_to_all | solution.py:81
  22.8 0.1 copy.31
  23.0 3.3 %collective-permute-start = (bf16[2,2,128]{1,2,0:T(8,128)(2,1)S(1)}, bf16[2,2,128]{1,2,0:T(8,128)(2,1)S(1)}, u32[]{:S(2)}, u32[]{:S(2)}) collective-permute-start(bf16[2,2,128]{1,2,0:T(8,128)(2,1)S(1)} %copy.31), channel_id=1, source_target_pairs={{0,8},{8,16},{16,24},{24,32},{32,40},{40,48},{48,56},{56,64},{64,7... | collective-permute-start | bytes 3080 | tf_op jit(solution)/shard_map/ppermute | solution.py:12
  26.3 1.0 copy.32
  27.3 1.0 copy.33
  28.3 1.3 convert_multiply_fusion.4
  29.6 0.0 copy-done.6
  29.6 0.0 copy-start.7
  29.6 2.0 %copy.30 = bf16[2048,128]{0,1:T(8,128)(2,1)} copy(bf16[2048,128]{1,0:T(8,128)(2,1)} %param.13) | data formatting | bytes 1048576 | tf_op args[0]
  31.7 13.7 %collective-permute-done = bf16[2,2,128]{1,2,0:T(8,128)(2,1)S(1)} collective-permute-done((bf16[2,2,128]{1,2,0:T(8,128)(2,1)S(1)}, bf16[2,2,128]{1,2,0:T(8,128)(2,1)S(1)}, u32[]{:S(2)}, u32[]{:S(2)}) %collective-permute-start) | collective-permute-done | bytes 1056 | tf_op jit(solution)/shard_map/ppermute | solution.py:12
  45.4 1.8 %bitcast_reduce_fusion = (f32[2048,2]{0,1:T(2,128)S(1)}, f32[2048,128]{0,1:T(8,128)S(1)}) fusion(f32[2048,128]{0,1:T(8,128)S(1)} %convert_multiply_fusion.4, f32[128]{0:T(128)S(1)} %get-tuple-element.9, f32[2,128]{0,1:T(8,128)S(1)} %multiply_bitcast_fusion, f32[128]{0:T(128)S(1)} %get-tuple-element.10, f32[128]{0:T(128)S(1)} %get-tuple-element.8, ...), kind=kLoop, calls=%fused_computation.35 | loop fusion | flops 2879488 | bytes 2640384 | tf_op jit(solution)/shard_map/reduce_sum | solution.py:57
  47.2 0.0 copy-done.7
  47.2 0.2 fusion.23
  47.4 0.8 copy.52
  48.2 4.7 %all-to-all-done.1 = bf16[128,4,2048]{2,1,0:T(4,128)(2,1)S(1)} async-done(((bf16[128,4,2048]{2,1,0:T(4,128)(2,1)}), bf16[128,4,2048]{2,1,0:T(4,128)(2,1)S(1)}, u32[]{:S(2)}, u32[]{:S(2)}) %all-to-all-start.1) | async-done | bytes 2097184 | tf_op jit(solution)/shard_map/all_to_all | solution.py:81
  52.9 5.0 %all-to-all-start = ((bf16[8,256,128]{1,2,0:T(8,128)(2,1)}), bf16[8,256,128]{1,2,0:T(8,128)(2,1)S(1)}, u32[]{:S(2)}, u32[]{:S(2)}) async-start(bf16[8,256,128]{1,2,0:T(8,128)(2,1)} %bitcast.71), calls=%async_computation | async-start | bytes 1048576 | tf_op jit(solution)/shard_map/all_to_all | solution.py:60
  57.9 2.0 %reshape.105 = bf16[512,2048]{1,0:T(8,128)(2,1)} reshape(bf16[128,4,2048]{2,1,0:T(4,128)(2,1)S(1)} %all-to-all-done.1) | data formatting | bytes 4194304 | tf_op jit(solution)/shard_map/reshape | solution.py:84
  59.9 6.6 %fusion.4 = f32[512,1024]{1,0:T(8,128)} fusion(bf16[512,2048]{1,0:T(8,128)(2,1)} %reshape.105, bf16[1,2048,1024]{2,1,0:T(8,128)(2,1)} %param.23), kind=kOutput, calls=%fused_computation.7 | convolution fusion | flops 2147483648 | bytes 8388608 | tf_op jit(solution)/shard_map/dot_general | solution.py:16
  66.5 9.9 %fusion.6 = bf16[512,2048]{1,0:T(8,128)(2,1)} fusion(bf16[1,1024,2048]{2,1,0:T(8,128)(2,1)} %param.25, f32[512,1024]{1,0:T(8,128)} %fusion.4, bf16[512,2048]{1,0:T(8,128)(2,1)S(1)} %copy-done.1, bf16[1,2048,1024]{2,1,0:T(8,128)(2,1)} %param.24), kind=kOutput, calls=%fused_computation.9 | convolution fusion | flops 4299161600 | bytes 14680064 | tf_op jit(solution)/shard_map/dot_general | solution.py:19
  76.4 4.1 %reshape.106 = bf16[128,4,2048]{2,1,0:T(4,128)(2,1)} reshape(bf16[512,2048]{1,0:T(8,128)(2,1)} %fusion.6) | data formatting | bytes 4194304 | tf_op jit(solution)/shard_map/reshape | solution.py:84
  80.5 0.0 all-to-all-done
  80.5 7.5 %all-to-all-start.2 = ((bf16[128,4,2048]{2,1,0:T(4,128)(2,1)}), bf16[128,4,2048]{2,1,0:T(4,128)(2,1)}, u32[]{:S(2)}, u32[]{:S(2)}) async-start(bf16[128,4,2048]{2,1,0:T(4,128)(2,1)} %reshape.106), calls=%async_computation.2 | async-start | bytes 4194304 | tf_op jit(solution)/shard_map/all_to_all | solution.py:83
  88.1 0.0 copy-done.5
  88.1 4.4 %convolution_convert_fusion = bf16[256,2048]{1,0:T(8,128)(2,1)} fusion(bf16[256,1024]{0,1:T(8,128)(2,1)S(1)} %bitcast.78, bf16[1024,2048]{1,0:T(8,128)(2,1)} %param.18), kind=kOutput, calls=%fused_computation.12 | convolution fusion | flops 1074266112 | bytes 5767168 | tf_op jit(solution)/shard_map/dot_general | solution.py:62
  92.5 25.3 %all-to-all-done.2 = bf16[128,4,2048]{2,1,0:T(4,128)(2,1)} async-done(((bf16[128,4,2048]{2,1,0:T(4,128)(2,1)}), bf16[128,4,2048]{2,1,0:T(4,128)(2,1)}, u32[]{:S(2)}, u32[]{:S(2)}) %all-to-all-start.2) | async-done | bytes 2097184 | tf_op jit(solution)/shard_map/all_to_all | solution.py:83
  117.8 2.5 %reshape.107 = bf16[512,2048]{1,0:T(8,128)(2,1)S(1)} reshape(bf16[128,4,2048]{2,1,0:T(4,128)(2,1)} %all-to-all-done.2) | data formatting | bytes 4194304 | tf_op jit(solution)/shard_map/reshape | solution.py:92
  120.3 3.3 %gather_fusion.1 = bf16[512,2048]{1,0:T(8,128)(2,1)} fusion(bf16[512,2048]{1,0:T(8,128)(2,1)S(1)} %reshape.107, s32[1024]{0:T(1024)S(1)} %pad_clamp_fusion), kind=kCustom, calls=%fused_computation.1 | custom fusion | bytes 4196352 | tf_op jit(solution)/shard_map/gather | solution.py:92
  123.7 3.2 %reshape.108 = bf16[256,2,2048]{2,1,0:T(2,128)(2,1)S(1)} reshape(bf16[512,2048]{1,0:T(8,128)(2,1)} %gather_fusion.1) | data formatting | bytes 4194304 | tf_op jit(solution)/shard_map/reshape | solution.py:92
  126.8 3.0 %fusion.38 = (bf16[256,1,2048]{2,1,0:T(2,128)(2,1)S(1)}, bf16[256,1,2048]{2,1,0:T(2,128)(2,1)S(1)}) fusion(bf16[256,2,2048]{2,1,0:T(2,128)(2,1)S(1)} %reshape.108), kind=kLoop, calls=%fused_computation.72 | loop fusion | bytes 4194304 | tf_op jit(solution)/shard_map/slice | solution.py:93
  129.8 3.3 %fusion.13 = bf16[256,2048]{1,0:T(8,128)(2,1)} fusion(bf16[256,1,2048]{2,1,0:T(2,128)(2,1)S(1)} %get-tuple-element.5, bf16[256,1,2048]{2,1,0:T(2,128)(2,1)S(1)} %get-tuple-element.4, f32[256]{0:T(256)S(1)} %bitcast.84, f32[256]{0:T(256)S(1)} %bitcast.83), kind=kLoop, calls=%fused_computation.18 | loop fusion | flops 3145728 | bytes 3147776 | tf_op jit(solution)/shard_map/convert_element_type | solution.py:95
  (26 shorter events, 0.2 us)
Async XLA Ops:
  0.6 5.3 %copy-start = (bf16[256,2048]{1,0:T(8,128)(2,1)S(1)}, bf16[256,2048]{1,0:T(8,128)(2,1)}, u32[]{:S(2)}) copy-start(bf16[256,2048]{1,0:T(8,128)(2,1)} %param.19) | copy-start | bytes 3145732
  0.6 5.6 %copy-start.4 = (f32[2048]{0:T(1024)S(1)}, f32[2048]{0:T(1024)}, u32[]{:S(2)}) copy-start(f32[2048]{0:T(1024)} %param.20) | copy-start | bytes 24580
  11.3 11.5 %copy-start.2 = (bf16[2048,128]{1,0:T(8,128)(2,1)S(1)}, bf16[2048,128]{1,0:T(8,128)(2,1)}, u32[]{:S(2)}) copy-start(bf16[2048,128]{1,0:T(8,128)(2,1)} %param.14) | copy-start | bytes 1572868
  11.3 11.5 %copy-start.3 = (bf16[2048,128]{1,0:T(8,128)(2,1)S(1)}, bf16[2048,128]{1,0:T(8,128)(2,1)}, u32[]{:S(2)}) copy-start(bf16[2048,128]{1,0:T(8,128)(2,1)} %param.15) | copy-start | bytes 1572868
  11.3 41.6 %all-to-all-start.1 = ((bf16[128,4,2048]{2,1,0:T(4,128)(2,1)}), bf16[128,4,2048]{2,1,0:T(4,128)(2,1)S(1)}, u32[]{:S(2)}, u32[]{:S(2)}) async-start(bf16[128,4,2048]{2,1,0:T(4,128)(2,1)} %reshape.104), calls=%async_computation.1 | async-start | bytes 4194304 | tf_op jit(solution)/shard_map/all_to_all | solution.py:81
  23.0 6.6 %copy-start.6 = (f32[3,128]{1,0:T(4,128)S(1)}, f32[3,128]{1,0:T(4,128)}, u32[]{:S(2)}) copy-start(f32[3,128]{1,0:T(4,128)} %param.16) | copy-start | bytes 4612
  23.0 22.4 %collective-permute-start = (bf16[2,2,128]{1,2,0:T(8,128)(2,1)S(1)}, bf16[2,2,128]{1,2,0:T(8,128)(2,1)S(1)}, u32[]{:S(2)}, u32[]{:S(2)}) collective-permute-start(bf16[2,2,128]{1,2,0:T(8,128)(2,1)S(1)} %copy.31), channel_id=1, source_target_pairs={{0,8},{8,16},{16,24},{24,32},{32,40},{40,48},{48,56},{56,64},{64,7... | collective-permute-start | bytes 3080 | tf_op jit(solution)/shard_map/ppermute | solution.py:12
  29.6 17.6 %copy-start.7 = (f32[128]{0:T(128)S(1)}, f32[128]{0:T(128)}, u32[]{:S(2)}) copy-start(f32[128]{0:T(128)} %param.17) | copy-start | bytes 1540
  52.9 27.6 %all-to-all-start = ((bf16[8,256,128]{1,2,0:T(8,128)(2,1)}), bf16[8,256,128]{1,2,0:T(8,128)(2,1)S(1)}, u32[]{:S(2)}, u32[]{:S(2)}) async-start(bf16[8,256,128]{1,2,0:T(8,128)(2,1)} %bitcast.71), calls=%async_computation | async-start | bytes 1048576 | tf_op jit(solution)/shard_map/all_to_all | solution.py:60
  59.9 6.6 %copy-start.1 = (bf16[512,2048]{1,0:T(8,128)(2,1)S(1)}, bf16[512,2048]{1,0:T(8,128)(2,1)}, u32[]{:S(2)}) copy-start(bf16[512,2048]{1,0:T(8,128)(2,1)} %reshape.105) | copy-start | bytes 6291460
  80.5 7.6 %copy-start.5 = (f32[256,2]{0,1:T(2,128)S(1)}, f32[256,2]{0,1:T(2,128)}, u32[]{:S(2)}) copy-start(f32[256,2]{0,1:T(2,128)} %param.22) | copy-start | bytes 6148
  80.5 37.3 %all-to-all-start.2 = ((bf16[128,4,2048]{2,1,0:T(4,128)(2,1)}), bf16[128,4,2048]{2,1,0:T(4,128)(2,1)}, u32[]{:S(2)}, u32[]{:S(2)}) async-start(bf16[128,4,2048]{2,1,0:T(4,128)(2,1)} %reshape.106), calls=%async_computation.2 | async-start | bytes 4194304 | tf_op jit(solution)/shard_map/all_to_all | solution.py:83
where the time goes:
time: 134 us; the launch traced here: 133 us
  waiting for transfers between devices  43.7 us (33%)
  local copies, waits for them, and re-layouts  31.9 us (24%)
  starting transfers between devices  27.2 us (20%)
  matrix products  21 us (16%)
  other arithmetic  8.4 us (6%)
    all_to_all x1, waiting for transfers between devices, shards(): lax.all_to_all(expert_rows(portion.reshape(-1, width), w_gate, w_up, w_do...  25.3 us
    ppermute x1, waiting for transfers between devices, shifted(): return lax.ppermute(value, axis, pairs)  13.7 us
    all_to_all x1, starting transfers between devices, shards(): lax.all_to_all(outgoing, ('ep', 'tp'), split_axis=0, concat_axis=0, tiled...  11.5 us
    dot_general x1, matrix products, expert_rows(): jnp.dot(hidden, w_down, preferred_element_type=jnp.float32)  9.92 us
    all_to_all x1, starting transfers between devices, shards(): lax.all_to_all(expert_rows(portion.reshape(-1, width), w_gate, w_up, w_do...  7.52 us
    dot_general x1, matrix products, expert_rows(): gate_part = jnp.dot(inputs, w_gate, preferred_element_type=jnp.float32)  6.63 us
    reshape x2, local copies, waits for them, and re-layouts, shards(): results = returned.reshape(-1, width)[target].reshape(tok_count, 2, width)  5.7 us
    unnamed x21, local copies, waits for them, and re-layouts  4.99 us
  transfers between devices with their start and end apart: 4, of which 3 were waited for; matrix products, arithmetic and copies ran while one was open for 27% of the time, Pallas kernels for 0%

commit v1 on v0

v1 whole, which is shorter than its diff:
```python
import functools

import jax
import jax.numpy as jnp
from jax import lax
from jax.experimental import pallas as pl
from jax.experimental.pallas import tpu as pltpu
from jax.sharding import PartitionSpec as P

MESH = pl.DeviceIdType.MESH
F32 = jnp.float32
BF16 = jnp.bfloat16
EPS = 1e-06

SIDE = 4
ORDER = (
    ((0, 0), (0, 1), (0, 3), (1, 0)),
    ((3, 3), (0, 2), (2, 0), (1, 2)),
    ((2, 1), (2, 3), (3, 2), (2, 2)),
    ((3, 0), (1, 1), (1, 3), (3, 1)),
)
OFFSETS = tuple(pair for chunk in ORDER for pair in chunk)
CHUNKS = len(ORDER)
PER_CHUNK = len(ORDER[0])
EP = len(OFFSETS)
TP = 8
GROUP_ROWS = 16
EXPERT_ROWS = 4
META = 128
TP_ORDER = (4, 5, 2, 3, 6, 7, 1)


def iota(shape, dim):
    return lax.broadcasted_iota(jnp.int32, shape, dim)


def hot(mask):
    return jnp.where(mask, 1.0, 0.0)


def dot(a, b, contract=((1,), (0,))):
    return lax.dot_general(a, b, (contract, ((), ())), preferred_element_type=F32)


def kernel(
    taps_ref,
    ggain_ref,
    mgain_ref,
    ids_ref,
    rw_ref,
    og_hbm,
    ig_hbm,
    ci_hbm,
    mixw_hbm,
    x_hbm,
    wg_hbm,
    wu_hbm,
    wd_hbm,
    mixed_hbm,
    moe_hbm,
    x_buf,
    xn_buf,
    og,
    ig,
    ci,
    edges,
    prod,
    normed,
    recvm,
    mixw,
    wg,
    wu,
    wd,
    perm,
    send1,
    recv1,
    send2,
    recv2,
    hid,
    send3,
    res,
    send4,
    ret,
    mixed_buf,
    moe_buf,
    load_sem,
    s1,
    r1,
    s2,
    r2,
    s3,
    r3,
    s4,
    r4,
    sm,
    rm,
    se,
    re,
    out_sem,
):
    ep = lax.axis_index("ep")
    tp = lax.axis_index("tp")
    z, x = ep // SIDE, ep % SIDE
    y, c = tp // 2, tp % 2
    width = x_buf.shape[1]
    tokens = x_buf.shape[0]

    def ep_peer(dz, dx):
        return (((z + dz) % SIDE) * SIDE + (x + dx) % SIDE, tp)

    def tp_peer(q, back=False):
        dy, dc = q // 2, q % 2
        dy = SIDE - dy if back else dy
        return (ep, ((y + dy) % SIDE) * 2 + (c + dc) % 2)

    def load(i, src, dst):
        cp = pltpu.make_async_copy(src, dst, load_sem.at[i])
        cp.start()
        return cp

    ld_x = load(0, x_hbm, x_buf)
    ld_ig = load(1, ig_hbm, ig)
    ld_ci = load(2, ci_hbm, ci)
    ld_og = load(3, og_hbm, og)
    ld_wg = load(4, wg_hbm.at[0], wg)
    ld_wu = load(5, wu_hbm.at[0], wu)
    ld_wd = load(6, wd_hbm.at[0], wd)
    ld_mw = load(7, mixw_hbm, mixw)

    barrier = pltpu.get_barrier_semaphore()
    for dz, dx in OFFSETS[1:]:
        pl.semaphore_signal(barrier, inc=1, device_id=ep_peer(dz, dx), device_id_type=MESH)
    for q in range(1, TP):
        pl.semaphore_signal(barrier, inc=1, device_id=tp_peer(q), device_id_type=MESH)

    sent = []

    def send(src, dst, ssem, rsem, device):
        cp = pltpu.make_async_remote_copy(
            src_ref=src, dst_ref=dst, send_sem=ssem, recv_sem=rsem, device_id=device, device_id_type=MESH
        )
        cp.start()
        sent.append(cp)
        return cp

    id0 = ids_ref[0:1, :]
    id1 = ids_ref[1:2, :]
    earlier = hot(iota((tokens, tokens), 0) < iota((tokens, tokens), 1)).astype(BF16)
    expert_of = iota((EP * TP, tokens), 0)
    hits0 = hot(expert_of == id0)
    hits1 = hot(expert_of == id1)
    before = dot((hits0 + hits1).astype(BF16), earlier)
    rank0 = jnp.sum(hits0 * before, axis=0, keepdims=True)
    rank1 = jnp.sum(hits1 * before, axis=0, keepdims=True)

    def base_slot(ids, rank):
        inner = ids & (TP - 1)
        dy = ((inner >> 1) - y) & (SIDE - 1)
        dc = ((inner & 1) + c) & 1
        return ((dy * 2 + dc) * GROUP_ROWS).astype(F32) + rank

    base0 = base_slot(id0, rank0)
    base1 = base_slot(id1, rank1)
    group = id0 >> 3
    place = (((group >> 2) - z) & 3) * SIDE + (((group & 3) - x) & 3)
    order = jnp.zeros_like(place)
    for k, (dz, dx) in enumerate(OFFSETS):
        order = jnp.where(place == dz * SIDE + dx, k, order)
    members = hot(iota((EP, tokens), 0) == order)
    group_rank = jnp.sum(members * dot(members.astype(BF16), earlier), axis=0, keepdims=True)
    slot = (order * GROUP_ROWS).astype(F32) + group_rank
    perm_f32 = hot(iota((tokens, tokens), 0).astype(F32) == slot)
    perm[...] = perm_f32.T.astype(BF16)
    forward = perm_f32.astype(BF16)
    w_hi = rw_ref[...].astype(BF16).astype(F32)
    w_lo = rw_ref[...] - w_hi
    meta_rows = jnp.concatenate(
        [base0, base1, w_hi[0:1], w_lo[0:1], w_hi[1:2], w_lo[1:2], jnp.zeros((META - 6, tokens), F32)], axis=0
    )
    meta = dot(forward, meta_rows.astype(BF16), ((1,), (1,))).astype(BF16)
    send1[:, width:] = meta
    recv1[0:GROUP_ROWS, width:] = meta[0:GROUP_ROWS]

    ld_x.wait()
    norm_rows = 32

    @pl.loop(0, tokens // norm_rows)
    def _(i):
        rows = pl.ds(pl.multiple_of(i * norm_rows, norm_rows), norm_rows)
        wide = x_buf[rows, :].astype(F32)
        scale = lax.rsqrt(jnp.mean(wide * wide, axis=-1, keepdims=True) + EPS)
        xn_buf[rows, :] = (wide * scale * mgain_ref[...]).astype(BF16)

    tile = 512

    @pl.loop(0, width // tile)
    def _(n):
        cols = pl.ds(pl.multiple_of(n * tile, tile), tile)
        moved = dot(forward, xn_buf[:, cols]).astype(BF16)
        send1[:, cols] = moved
        recv1[0:GROUP_ROWS, cols] = moved[0:GROUP_ROWS]

    ld_ig.wait()
    ld_ci.wait()
    pl.semaphore_wait(barrier, EP - 1 + TP - 1)

    length = ig.shape[0]
    after = (lax.rem(ep + 1, EP), tp)
    edge = [
        send(src.at[pl.ds(length - 16, 16)], edges.at[i], se.at[i], re.at[i], after)
        for i, src in enumerate((ig, ci))
    ]
    first = []
    for k in range(1, EP):
        rows = pl.ds(k * GROUP_ROWS, GROUP_ROWS)
        first.append(send(send1.at[rows], recv1.at[rows], s1.at[k], r1.at[k], ep_peer(*OFFSETS[k])))

    for cp in edge:
        cp.wait_recv()
    ld_og.wait()
    keep = jnp.where(ep > 0, 1.0, 0.0)
    prod[0:8, :] = edges[0].astype(F32)[8:16] * edges[1].astype(F32)[8:16] * keep
    step_rows = tokens

    @pl.loop(0, length // step_rows)
    def _(i):
        rows = pl.ds(pl.multiple_of(i * step_rows, step_rows), step_rows)
        prod[pl.ds(pl.multiple_of(i * step_rows + 8, 8), step_rows), :] = ig[rows, :].astype(F32) * ci[rows, :].astype(F32)

    same = hot((iota((META, META), 0) >> 6) == (iota((META, META), 1) >> 6))
    averager = (same * (1.0 / 64.0)).astype(BF16)

    @pl.loop(0, length // step_rows)
    def _(i):
        rows = pl.ds(pl.multiple_of(i * step_rows, step_rows), step_rows)
        block = prod[pl.ds(pl.multiple_of(i * step_rows, 8), step_rows + 8), :]
        convolved = (
            taps_ref[0:1, :] * pltpu.roll(block, 2, 0)[8:]
            + taps_ref[1:2, :] * pltpu.roll(block, 1, 0)[8:]
            + taps_ref[2:3, :] * block[8:]
        )
        gated = og[rows, :].astype(F32) * convolved
        square = gated * gated
        high = square.astype(BF16)
        low = (square - high.astype(F32)).astype(BF16)
        inv = lax.rsqrt(dot(high, averager) + dot(low, averager) + EPS)
        normed[rows, :] = (gated * inv * ggain_ref[...]).astype(BF16)

    own = pl.ds(pl.multiple_of(tp * tokens, tokens), tokens)
    recvm[tp] = normed[own, :]
    mix = []
    for q in TP_ORDER:
        peer = tp_peer(q)
        rows = pl.ds(pl.multiple_of(peer[1] * tokens, tokens), tokens)
        mix.append(send(normed.at[rows], recvm.at[tp], sm.at[q], rm.at[q], peer))

    chunk_in = PER_CHUNK * GROUP_ROWS
    chunk_out = TP * GROUP_ROWS

    def places(j):
        info = recv1[j * chunk_in : (j + 1) * chunk_in, width:].astype(F32)
        shift = ((iota((chunk_in, chunk_out), 0) >> 4) * EXPERT_ROWS).astype(F32)
        lane = iota((chunk_in, chunk_out), 1).astype(F32)
        return info, info[:, 0:1] + shift == lane, info[:, 1:2] + shift == lane

    second = []
    for j in range(CHUNKS):
        for k in range(max(1, j * PER_CHUNK), (j + 1) * PER_CHUNK):
            first[k - 1].wait_recv()
        _, at0, at1 = places(j)
        split = (hot(at0) + hot(at1)).T.astype(BF16)
        base = j * chunk_out

        @pl.loop(0, width // tile)
        def _(n):
            cols = pl.ds(pl.multiple_of(n * tile, tile), tile)
            moved = dot(split, recv1[j * chunk_in : (j + 1) * chunk_in, cols]).astype(BF16)
            send2[base : base + chunk_out, cols] = moved
            recv2[base : base + GROUP_ROWS, cols] = moved[0:GROUP_ROWS]

        arrivals = []
        for q in TP_ORDER:
            rows = pl.ds(base + q * GROUP_ROWS, GROUP_ROWS)
            arrivals.append(send(send2.at[rows], recv2.at[rows], s2.at[j, q], r2.at[j, q], tp_peer(q)))
        second.append(arrivals)

    ld_wg.wait()
    ld_wu.wait()
    ld_wd.wait()
    hidden_units = wg.shape[1]
    hid_tile = 256
    third = []
    for j in range(CHUNKS):
        for cp in second[j]:
            cp.wait_recv()
        base = j * chunk_out

        @pl.loop(0, hidden_units // hid_tile)
        def _(n):
            cols = pl.ds(pl.multiple_of(n * hid_tile, hid_tile), hid_tile)
            inputs = recv2[base : base + chunk_out, :]
            gate = dot(inputs, wg[:, cols])
            up = dot(inputs, wu[:, cols])
            hid[:, cols] = (gate / (1.0 + jnp.exp(-gate)) * up).astype(BF16)

        @pl.loop(0, width // tile)
        def _(n):
            cols = pl.ds(pl.multiple_of(n * tile, tile), tile)
            result = dot(hid[...], wd[:, cols]).astype(BF16)
            send3[base : base + chunk_out, cols] = result
            res[base : base + GROUP_ROWS, cols] = result[0:GROUP_ROWS]

        arrivals = []
        for q in TP_ORDER:
            rows = pl.ds(base + q * GROUP_ROWS, GROUP_ROWS)
            arrivals.append(send(send3.at[rows], res.at[rows], s3.at[j, q], r3.at[j, q], tp_peer(q, back=True)))
        third.append(arrivals)

    ld_mw.wait()
    for cp in mix:
        cp.wait_recv()

    @pl.loop(0, width // tile)
    def _(n):
        cols = pl.ds(pl.multiple_of(n * tile, tile), tile)
        total = jnp.zeros((tokens, tile), F32)
        for i in range(0, TP, 2):
            pair = jnp.concatenate([recvm[i], recvm[i + 1]], axis=1)
            total += dot(pair, mixw[i * META : (i + 2) * META, cols])
        mixed_buf[:, cols] = total.astype(BF16)

    out_mixed = pltpu.make_async_copy(mixed_buf, mixed_hbm, out_sem.at[0])
    out_mixed.start()

    last = []
    for j in range(CHUNKS):
        for cp in third[j]:
            cp.wait_recv()
        info, at0, at1 = places(j)
        high = (jnp.where(at0, info[:, 2:3], 0.0) + jnp.where(at1, info[:, 4:5], 0.0)).astype(BF16)
        low = (jnp.where(at0, info[:, 3:4], 0.0) + jnp.where(at1, info[:, 5:6], 0.0)).astype(BF16)
        base = j * chunk_in

        @pl.loop(0, width // tile)
        def _(n):
            cols = pl.ds(pl.multiple_of(n * tile, tile), tile)
            results = res[j * chunk_out : (j + 1) * chunk_out, cols]
            joined = (dot(high, results) + dot(low, results)).astype(BF16)
            send4[base : base + chunk_in, cols] = joined
            if j == 0:
                ret[0:GROUP_ROWS, cols] = joined[0:GROUP_ROWS]

        for k in range(max(1, j * PER_CHUNK), (j + 1) * PER_CHUNK):
            dz, dx = OFFSETS[k]
            rows = pl.ds(k * GROUP_ROWS, GROUP_ROWS)
            last.append(send(send4.at[rows], ret.at[rows], s4.at[k], r4.at[k], ep_peer(SIDE - dz, SIDE - dx)))

    for cp in last:
        cp.wait_recv()

    @pl.loop(0, width // tile)
    def _(n):
        cols = pl.ds(pl.multiple_of(n * tile, tile), tile)
        moe_buf[:, cols] = dot(perm[...], ret[:, cols]).astype(BF16)

    out_moe = pltpu.make_async_copy(moe_buf, moe_hbm, out_sem.at[1])
    out_moe.start()
    for cp in sent:
        cp.wait_send()
    out_mixed.wait()
    out_moe.wait()


def shards(
    out_gate, in_gate, conv_input, conv_taps, group_gain, mix_out_w, moe_in, moe_gain, route_ids, route_weight,
    gate_w, up_w, down_w,
):
    rows, channels = in_gate.shape
    tokens, width = moe_in.shape
    hidden = gate_w.shape[2]
    vmem = pl.BlockSpec(memory_space=pltpu.VMEM)
    hbm = pl.BlockSpec(memory_space=pl.ANY)
    dma = pltpu.SemaphoreType.DMA
    out = jax.ShapeDtypeStruct((tokens, width), BF16)
    V = pltpu.VMEM
    slots = 2 * tokens
    return pl.pallas_call(
        kernel,
        out_shape=(out, out),
        in_specs=[vmem] * 5 + [hbm] * 8,
        out_specs=(hbm, hbm),
        scratch_shapes=[
            V((tokens, width), BF16),
            V((tokens, width), BF16),
            V((rows, channels), BF16),
            V((rows, channels), BF16),
            V((rows, channels), BF16),
            V((2, 16, channels), BF16),
            V((rows + 8, channels), F32),
            V((rows, channels), BF16),
            V((TP, tokens, channels), BF16),
            V(mix_out_w.shape, BF16),
            V((width, hidden), BF16),
            V((width, hidden), BF16),
            V((hidden, width), BF16),
            V((tokens, tokens), BF16),
            V((tokens, width + META), BF16),
            V((tokens, width + META), BF16),
            V((slots, width), BF16),
            V((slots, width), BF16),
            V((TP * GROUP_ROWS, hidden), BF16),
            V((slots, width), BF16),
            V((slots, width), BF16),
            V((tokens, width), BF16),
            V((tokens, width), BF16),
            V((tokens, width), BF16),
            V((tokens, width), BF16),
            dma((8,)),
            dma((EP,)), dma((EP,)),
            dma((CHUNKS, TP)), dma((CHUNKS, TP)),
            dma((CHUNKS, TP)), dma((CHUNKS, TP)),
            dma((EP,)), dma((EP,)),
            dma((TP,)), dma((TP,)),
            dma((2,)), dma((2,)),
            dma((2,)),
        ],
        compiler_params=pltpu.CompilerParams(
            collective_id=0, has_side_effects=True, vmem_limit_bytes=60 * 1024 * 1024
        ),
    )(
        conv_taps, group_gain.reshape(1, -1), moe_gain.reshape(1, -1), route_ids.T, route_weight.T,
        out_gate, in_gate, conv_input, mix_out_w, moe_in, gate_w, up_w, down_w,
    )


def solution(mesh):
    both = ("ep", "tp")
    in_specs = (
        P("ep", "tp"), P("ep", "tp"), P("ep", "tp"), P(None, "tp"), P("tp"), P(),
        P(both, None), P(), P(both, None), P(both, None),
        P(both, None, None), P(both, None, None), P(both, None, None),
    )
    return jax.shard_map(
        shards, mesh=mesh, in_specs=in_specs, out_specs=(P(both, None), P(both, None)), check_vma=False
    )
```

time: 134 us -> 83.5 us (0.62)
  Pallas kernels: 0 us -> 78.1 us
  waiting for transfers between devices: 43.7 us -> 0 us
  local copies, waits for them, and re-layouts: 31.9 us -> 4.61 us
  starting transfers between devices: 27.2 us -> 0 us
  matrix products: 21 us -> 0 us
  other arithmetic: 8.4 us -> 0 us
    pallas_call x0 -> x1, Pallas kernels: none -> 78.1 us  [shards(): pl.pallas_call(kernel, out_shape=(out, out), in_specs=[vmem] * 5 + [hbm]...]
    all_to_all x3 -> x0, waiting for transfers between devices: 30 us -> none  [the longest x1 25.3 us: shards(): lax.all_to_all(expert_rows(portion.reshape(-1, width), w_gate, w_up, w_do...]
    all_to_all x3 -> x0, starting transfers between devices: 24 us -> none  [the longest x1 11.5 us: shards(): lax.all_to_all(outgoing, ('ep', 'tp'), split_axis=0, concat_axis=0, tiled...]
    dot_general x3 -> x0, matrix products: 21 us -> none  [the longest x1 9.92 us: expert_rows(): jnp.dot(hidden, w_down, preferred_element_type=jnp.float32)]
    reshape x6 -> x0, local copies, waits for them, and re-layouts: 14.8 us -> none  [the longest x2 5.7 us: shards(): results = returned.reshape(-1, width)[target].reshape(tok_count, 2, width)]
    ppermute x1 -> x0, waiting for transfers between devices: 13.7 us -> none  [shifted(): return lax.ppermute(value, axis, pairs)]
    gather x2 -> x0, local copies, waits for them, and re-layouts: 5.79 us -> none  [the longest x1 3.33 us: shards(): results = returned.reshape(-1, width)[target].reshape(tok_count, 2, width)]
    convert_element_type x3 -> x0, other arithmetic: 3.78 us -> none  [the longest x1 3.3 us: shards(): (first_out * route_weight[:, 0:1] + second * route_weight[:, 1:2]).astype...]
  transfers between devices with their start and end apart: 4 -> 0, of which waited for: 3 -> 0; matrix products, arithmetic and copies ran while one was open for 27% -> 0% of each run, Pallas kernels for 0% -> 0%
where the time goes in v1:
time: 83.5 us; the launch traced here: 83.3 us
  Pallas kernels  78.1 us (94%)
  local copies, waits for them, and re-layouts  4.61 us (6%)
    pallas_call x1, Pallas kernels, shards(): pl.pallas_call(kernel, out_shape=(out, out), in_specs=[vmem] * 5 + [hbm]...  78.1 us
    unnamed x2, local copies, waits for them, and re-layouts  4.61 us

profile of v1, /device:TPU:1, one launch (start us, length us, event | category | flops | bytes accessed | tf_op | source)
XLA Modules:
  0.0 83.3 jit_solution(7483723887029018563)
XLA Ops:
  0.6 78.1 %shard_map.140 = (bf16[256,2048]{1,0:T(8,128)(2,1)}, bf16[256,2048]{1,0:T(8,128)(2,1)}) custom-call(f32[3,128]{1,0:T(4,128)} %taps_ref.1, f32[1,128]{1,0:T(1,128)} %bitcast.7, f32[1,2048]{1,0:T(1,128)} %bitcast.4, s32[2,256]{1,0:T(2,128)} %bitcast.5, f32[2,256]{1,0:T(2,128)} %bitcast.6, bf16[2048,128]{1,0:T(8,128)(2,1)} %og_hbm.1, bf16[2048,128]{1,0:T(8,128)(2,1)} %ig_hbm.1, ...), custom_call_target="tpu_custom_call" | custom-call | tf_op jit(solution)/shard_map/pallas_call | solution.py:387
  78.7 2.3 %copy.17 = bf16[256,2048]{1,0:T(8,128)(2,1)} copy(bf16[256,2048]{1,0:T(8,128)(2,1)} %get-tuple-element.4) | data formatting | bytes 2097152
  81.0 2.3 %copy.18 = bf16[256,2048]{1,0:T(8,128)(2,1)} copy(bf16[256,2048]{1,0:T(8,128)(2,1)} %get-tuple-element.5) | data formatting | bytes 2097152

commit v2 on v1

--- a/solution.py
+++ b/solution.py
@@ -14,13 +14,15 @@
 
 SIDE = 4
 ORDER = (
-    ((0, 0), (0, 1), (0, 3), (1, 0)),
-    ((3, 3), (0, 2), (2, 0), (1, 2)),
-    ((2, 1), (2, 3), (3, 2), (2, 2)),
-    ((3, 0), (1, 1), (1, 3), (3, 1)),
+    ((1, 2), (2, 1), (0, 2), (2, 0)),
+    ((2, 2), (2, 3), (3, 2), (1, 1)),
+    ((3, 0), (1, 3), (3, 1), (3, 3)),
+    ((0, 0), (0, 1), (1, 0), (0, 3)),
 )
 OFFSETS = tuple(pair for chunk in ORDER for pair in chunk)
 CHUNKS = len(ORDER)
+SELF = OFFSETS.index((0, 0))
+SPLIT_ORDER = (3, 0, 1, 2)
 PER_CHUNK = len(ORDER[0])
 EP = len(OFFSETS)
 TP = 8
@@ -28,6 +30,12 @@
 EXPERT_ROWS = 4
 META = 128
 TP_ORDER = (4, 5, 2, 3, 6, 7, 1)
+MIX_EARLY = (4, 5, 1)
+MIX_LATE = (2, 3, 6, 7)
+
+
+def chunk_peers(j):
+    return [k for k in range(j * PER_CHUNK, (j + 1) * PER_CHUNK) if k != SELF]
 
 
 def iota(shape, dim):
@@ -43,11 +51,11 @@
 
 
 def kernel(
-    taps_ref,
-    ggain_ref,
-    mgain_ref,
-    ids_ref,
-    rw_ref,
+    taps_hbm,
+    ggain_hbm,
+    mgain_hbm,
+    ids_hbm,
+    rw_hbm,
     og_hbm,
     ig_hbm,
     ci_hbm,
@@ -57,7 +65,13 @@
     wu_hbm,
     wd_hbm,
     mixed_hbm,
-    moe_hbm,
+    ret_hbm,
+    perm_hbm,
+    taps_ref,
+    ggain_ref,
+    mgain_ref,
+    ids_ref,
+    rw_ref,
     x_buf,
     xn_buf,
     og,
@@ -80,9 +94,8 @@
     send3,
     res,
     send4,
-    ret,
+    mixed_sum,
     mixed_buf,
-    moe_buf,
     load_sem,
     s1,
     r1,
@@ -97,6 +110,7 @@
     se,
     re,
     out_sem,
+    mix_sem,
 ):
     ep = lax.axis_index("ep")
     tp = lax.axis_index("tp")
@@ -118,17 +132,25 @@
         cp.start()
         return cp
 
+    ld_ids = load(8, ids_hbm, ids_ref)
+    ld_rw = load(9, rw_hbm, rw_ref)
     ld_x = load(0, x_hbm, x_buf)
+    ld_mgain = load(10, mgain_hbm, mgain_ref)
     ld_ig = load(1, ig_hbm, ig)
     ld_ci = load(2, ci_hbm, ci)
     ld_og = load(3, og_hbm, og)
+    ld_taps = load(11, taps_hbm, taps_ref)
+    ld_ggain = load(12, ggain_hbm, ggain_ref)
     ld_wg = load(4, wg_hbm.at[0], wg)
     ld_wu = load(5, wu_hbm.at[0], wu)
     ld_wd = load(6, wd_hbm.at[0], wd)
     ld_mw = load(7, mixw_hbm, mixw)
 
     barrier = pltpu.get_barrier_semaphore()
-    for dz, dx in OFFSETS[1:]:
+    for k in range(EP):
+        if k == SELF:
+            continue
+        dz, dx = OFFSETS[k]
         pl.semaphore_signal(barrier, inc=1, device_id=ep_peer(dz, dx), device_id_type=MESH)
     for q in range(1, TP):
         pl.semaphore_signal(barrier, inc=1, device_id=tp_peer(q), device_id_type=MESH)
@@ -143,6 +165,8 @@
         sent.append(cp)
         return cp
 
+    ld_ids.wait()
+    ld_rw.wait()
     id0 = ids_ref[0:1, :]
     id1 = ids_ref[1:2, :]
     earlier = hot(iota((tokens, tokens), 0) < iota((tokens, tokens), 1)).astype(BF16)
@@ -171,6 +195,8 @@
     slot = (order * GROUP_ROWS).astype(F32) + group_rank
     perm_f32 = hot(iota((tokens, tokens), 0).astype(F32) == slot)
     perm[...] = perm_f32.T.astype(BF16)
+    out_perm = pltpu.make_async_copy(perm, perm_hbm, out_sem.at[1])
+    out_perm.start()
     forward = perm_f32.astype(BF16)
     w_hi = rw_ref[...].astype(BF16).astype(F32)
     w_lo = rw_ref[...] - w_hi
@@ -179,9 +205,11 @@
     )
     meta = dot(forward, meta_rows.astype(BF16), ((1,), (1,))).astype(BF16)
     send1[:, width:] = meta
-    recv1[0:GROUP_ROWS, width:] = meta[0:GROUP_ROWS]
+    mine = slice(SELF * GROUP_ROWS, (SELF + 1) * GROUP_ROWS)
+    recv1[mine, width:] = meta[mine]
 
     ld_x.wait()
+    ld_mgain.wait()
     norm_rows = 32
 
     @pl.loop(0, tokens // norm_rows)
@@ -198,7 +226,7 @@
         cols = pl.ds(pl.multiple_of(n * tile, tile), tile)
         moved = dot(forward, xn_buf[:, cols]).astype(BF16)
         send1[:, cols] = moved
-        recv1[0:GROUP_ROWS, cols] = moved[0:GROUP_ROWS]
+        recv1[mine, cols] = moved[mine]
 
     ld_ig.wait()
     ld_ci.wait()
@@ -210,30 +238,27 @@
         send(src.at[pl.ds(length - 16, 16)], edges.at[i], se.at[i], re.at[i], after)
         for i, src in enumerate((ig, ci))
     ]
-    first = []
-    for k in range(1, EP):
-        rows = pl.ds(k * GROUP_ROWS, GROUP_ROWS)
-        first.append(send(send1.at[rows], recv1.at[rows], s1.at[k], r1.at[k], ep_peer(*OFFSETS[k])))
-
-    for cp in edge:
-        cp.wait_recv()
+    first = {}
+    for j in SPLIT_ORDER:
+        for k in chunk_peers(j):
+            rows = pl.ds(k * GROUP_ROWS, GROUP_ROWS)
+            first[k] = send(send1.at[rows], recv1.at[rows], s1.at[k], r1.at[k], ep_peer(*OFFSETS[k]))
+
     ld_og.wait()
-    keep = jnp.where(ep > 0, 1.0, 0.0)
-    prod[0:8, :] = edges[0].astype(F32)[8:16] * edges[1].astype(F32)[8:16] * keep
-    step_rows = tokens
-
-    @pl.loop(0, length // step_rows)
+    ld_taps.wait()
+    ld_ggain.wait()
+
+    @pl.loop(0, length // tokens)
     def _(i):
-        rows = pl.ds(pl.multiple_of(i * step_rows, step_rows), step_rows)
-        prod[pl.ds(pl.multiple_of(i * step_rows + 8, 8), step_rows), :] = ig[rows, :].astype(F32) * ci[rows, :].astype(F32)
+        rows = pl.ds(pl.multiple_of(i * tokens, tokens), tokens)
+        prod[pl.ds(pl.multiple_of(i * tokens + 8, 8), tokens), :] = ig[rows, :].astype(F32) * ci[rows, :].astype(F32)
 
     same = hot((iota((META, META), 0) >> 6) == (iota((META, META), 1) >> 6))
     averager = (same * (1.0 / 64.0)).astype(BF16)
 
-    @pl.loop(0, length // step_rows)
-    def _(i):
-        rows = pl.ds(pl.multiple_of(i * step_rows, step_rows), step_rows)
-        block = prod[pl.ds(pl.multiple_of(i * step_rows, 8), step_rows + 8), :]
+    def convolve(i):
+        rows = pl.ds(pl.multiple_of(i * tokens, tokens), tokens)
+        block = prod[pl.ds(pl.multiple_of(i * tokens, 8), tokens + 8), :]
         convolved = (
             taps_ref[0:1, :] * pltpu.roll(block, 2, 0)[8:]
             + taps_ref[1:2, :] * pltpu.roll(block, 1, 0)[8:]
@@ -246,13 +271,21 @@
         inv = lax.rsqrt(dot(high, averager) + dot(low, averager) + EPS)
         normed[rows, :] = (gated * inv * ggain_ref[...]).astype(BF16)
 
-    own = pl.ds(pl.multiple_of(tp * tokens, tokens), tokens)
-    recvm[tp] = normed[own, :]
-    mix = []
-    for q in TP_ORDER:
+    pl.loop(1, length // tokens)(convolve)
+    for cp in edge:
+        cp.wait_recv()
+    keep = jnp.where(ep > 0, 1.0, 0.0)
+    prod[0:8, :] = edges[0].astype(F32)[8:16] * edges[1].astype(F32)[8:16] * keep
+    convolve(0)
+
+    recvm[tp] = normed[pl.ds(pl.multiple_of(tp * tokens, tokens), tokens), :]
+
+    def send_mixer(q):
         peer = tp_peer(q)
         rows = pl.ds(pl.multiple_of(peer[1] * tokens, tokens), tokens)
-        mix.append(send(normed.at[rows], recvm.at[tp], sm.at[q], rm.at[q], peer))
+        return send(normed.at[rows], recvm.at[tp], sm.at[q], rm.at[q], peer)
+
+    mix_early = [send_mixer(q) for q in MIX_EARLY]
 
     chunk_in = PER_CHUNK * GROUP_ROWS
     chunk_out = TP * GROUP_ROWS
@@ -263,10 +296,10 @@
         lane = iota((chunk_in, chunk_out), 1).astype(F32)
         return info, info[:, 0:1] + shift == lane, info[:, 1:2] + shift == lane
 
-    second = []
-    for j in range(CHUNKS):
-        for k in range(max(1, j * PER_CHUNK), (j + 1) * PER_CHUNK):
-            first[k - 1].wait_recv()
+    second = {}
+    for j in SPLIT_ORDER:
+        for k in chunk_peers(j):
+            first[k].wait_recv()
         _, at0, at1 = places(j)
         split = (hot(at0) + hot(at1)).T.astype(BF16)
         base = j * chunk_out
@@ -282,7 +315,7 @@
         for q in TP_ORDER:
             rows = pl.ds(base + q * GROUP_ROWS, GROUP_ROWS)
             arrivals.append(send(send2.at[rows], recv2.at[rows], s2.at[j, q], r2.at[j, q], tp_peer(q)))
-        second.append(arrivals)
+        second[j] = arrivals
 
     ld_wg.wait()
     ld_wu.wait()
@@ -316,21 +349,22 @@
             arrivals.append(send(send3.at[rows], res.at[rows], s3.at[j, q], r3.at[j, q], tp_peer(q, back=True)))
         third.append(arrivals)
 
+    mix_late = [send_mixer(q) for q in MIX_LATE]
+
+    def chip_part(dy, cols):
+        chip = (y + dy) % SIDE
+        pair = jnp.concatenate([recvm[chip * 2], recvm[chip * 2 + 1]], axis=1)
+        weights = mixw[pl.ds(pl.multiple_of(chip * (2 * META), 2 * META), 2 * META), cols]
+        return dot(pair, weights)
+
     ld_mw.wait()
-    for cp in mix:
+    for cp in mix_early:
         cp.wait_recv()
 
     @pl.loop(0, width // tile)
     def _(n):
         cols = pl.ds(pl.multiple_of(n * tile, tile), tile)
-        total = jnp.zeros((tokens, tile), F32)
-        for i in range(0, TP, 2):
-            pair = jnp.concatenate([recvm[i], recvm[i + 1]], axis=1)
-            total += dot(pair, mixw[i * META : (i + 2) * META, cols])
-        mixed_buf[:, cols] = total.astype(BF16)
-
-    out_mixed = pltpu.make_async_copy(mixed_buf, mixed_hbm, out_sem.at[0])
-    out_mixed.start()
+        mixed_sum[:, cols] = chip_part(0, cols) + chip_part(2, cols)
 
     last = []
     for j in range(CHUNKS):
@@ -347,28 +381,62 @@
             results = res[j * chunk_out : (j + 1) * chunk_out, cols]
             joined = (dot(high, results) + dot(low, results)).astype(BF16)
             send4[base : base + chunk_in, cols] = joined
-            if j == 0:
-                ret[0:GROUP_ROWS, cols] = joined[0:GROUP_ROWS]
-
-        for k in range(max(1, j * PER_CHUNK), (j + 1) * PER_CHUNK):
+
+        for k in chunk_peers(j):
             dz, dx = OFFSETS[k]
             rows = pl.ds(k * GROUP_ROWS, GROUP_ROWS)
-            last.append(send(send4.at[rows], ret.at[rows], s4.at[k], r4.at[k], ep_peer(SIDE - dz, SIDE - dx)))
-
+            last.append(send(send4.at[rows], ret_hbm.at[rows], s4.at[k], r4.at[k], ep_peer(SIDE - dz, SIDE - dx)))
+
+    home = pl.ds(SELF * GROUP_ROWS, GROUP_ROWS)
+    own = pltpu.make_async_copy(send4.at[home], ret_hbm.at[home], out_sem.at[0])
+    own.start()
+
+    for cp in mix_late:
+        cp.wait_recv()
+    outs = []
+    for n in range(width // tile):
+        cols = slice(n * tile, (n + 1) * tile)
+        mixed_buf[:, cols] = (mixed_sum[:, cols] + chip_part(1, cols) + chip_part(3, cols)).astype(BF16)
+        cp = pltpu.make_async_copy(mixed_buf.at[:, cols], mixed_hbm.at[:, cols], mix_sem.at[n])
+        cp.start()
+        outs.append(cp)
+
+    for cp in sent:
+        cp.wait_send()
+    for cp in outs:
+        cp.wait()
+    own.wait()
+    out_perm.wait()
     for cp in last:
         cp.wait_recv()
 
-    @pl.loop(0, width // tile)
-    def _(n):
-        cols = pl.ds(pl.multiple_of(n * tile, tile), tile)
-        moe_buf[:, cols] = dot(perm[...], ret[:, cols]).astype(BF16)
-
-    out_moe = pltpu.make_async_copy(moe_buf, moe_hbm, out_sem.at[1])
-    out_moe.start()
-    for cp in sent:
-        cp.wait_send()
-    out_mixed.wait()
-    out_moe.wait()
+
+def finish(perm_hbm, ret_hbm, mixed_hbm, out_mixed, out_moe, perm, ret, mixed, moe, in_sem, out_sem):
+    tokens, width = ret.shape
+    steps = in_sem.shape[1]
+    tile = width // steps
+    ld_perm = pltpu.make_async_copy(perm_hbm, perm, in_sem.at[2, 0])
+    ld_perm.start()
+    cols = [slice(n * tile, (n + 1) * tile) for n in range(steps)]
+
+    def copies(src, dst, sem):
+        return [pltpu.make_async_copy(src.at[:, cols[n]], dst.at[:, cols[n]], sem.at[n]) for n in range(steps)]
+
+    rows_in = copies(ret_hbm, ret, in_sem.at[0])
+    mixed_in = copies(mixed_hbm, mixed, in_sem.at[1])
+    moe_out = copies(moe, out_moe, out_sem.at[0])
+    mixed_out = copies(mixed, out_mixed, out_sem.at[1])
+    for cp in rows_in + mixed_in:
+        cp.start()
+    ld_perm.wait()
+    for n in range(steps):
+        rows_in[n].wait()
+        moe[:, cols[n]] = dot(perm[...], ret[:, cols[n]]).astype(BF16)
+        moe_out[n].start()
+        mixed_in[n].wait()
+        mixed_out[n].start()
+    for cp in moe_out + mixed_out:
+        cp.wait()
 
 
 def shards(
@@ -378,18 +446,23 @@
     rows, channels = in_gate.shape
     tokens, width = moe_in.shape
     hidden = gate_w.shape[2]
-    vmem = pl.BlockSpec(memory_space=pltpu.VMEM)
     hbm = pl.BlockSpec(memory_space=pl.ANY)
     dma = pltpu.SemaphoreType.DMA
     out = jax.ShapeDtypeStruct((tokens, width), BF16)
     V = pltpu.VMEM
     slots = 2 * tokens
-    return pl.pallas_call(
+    square = jax.ShapeDtypeStruct((tokens, tokens), BF16)
+    mixed, returned, perm = pl.pallas_call(
         kernel,
-        out_shape=(out, out),
-        in_specs=[vmem] * 5 + [hbm] * 8,
-        out_specs=(hbm, hbm),
+        out_shape=(out, out, square),
+        in_specs=[hbm] * 13,
+        out_specs=(hbm, hbm, hbm),
         scratch_shapes=[
+            V(conv_taps.shape, F32),
+            V((1, channels), F32),
+            V((1, width), F32),
+            V((2, tokens), jnp.int32),
+            V((2, tokens), F32),
             V((tokens, width), BF16),
             V((tokens, width), BF16),
             V((rows, channels), BF16),
@@ -412,10 +485,9 @@
             V((slots, width), BF16),
             V((slots, width), BF16),
             V((tokens, width), BF16),
-            V((tokens, width), BF16),
-            V((tokens, width), BF16),
-            V((tokens, width), BF16),
-            dma((8,)),
+            V((tokens, width), F32),
+            V((tokens, width), BF16),
+            dma((13,)),
             dma((EP,)), dma((EP,)),
             dma((CHUNKS, TP)), dma((CHUNKS, TP)),
             dma((CHUNKS, TP)), dma((CHUNKS, TP)),
@@ -423,6 +495,7 @@
             dma((TP,)), dma((TP,)),
             dma((2,)), dma((2,)),
             dma((2,)),
+            dma((4,)),
         ],
         compiler_params=pltpu.CompilerParams(
             collective_id=0, has_side_effects=True, vmem_limit_bytes=60 * 1024 * 1024
@@ -431,6 +504,21 @@
         conv_taps, group_gain.reshape(1, -1), moe_gain.reshape(1, -1), route_ids.T, route_weight.T,
         out_gate, in_gate, conv_input, mix_out_w, moe_in, gate_w, up_w, down_w,
     )
+    steps = 4
+    return pl.pallas_call(
+        finish,
+        out_shape=(out, out),
+        in_specs=[hbm] * 3,
+        out_specs=(hbm, hbm),
+        scratch_shapes=[
+            V((tokens, tokens), BF16),
+            V((tokens, width), BF16),
+            V((tokens, width), BF16),
+            V((tokens, width), BF16),
+            dma((3, steps)),
+            dma((2, steps)),
+        ],
+    )(perm, returned, mixed)
 
 
 def solution(mesh):

time: 83.5 us -> 75.1 us (0.90)
  local copies, waits for them, and re-layouts: 4.61 us -> 0 us
  Pallas kernels: 78.1 us -> 74.3 us
    unnamed x2 -> x0, local copies, waits for them, and re-layouts: 4.61 us -> none
    pallas_call x1 -> x2, Pallas kernels: 78.1 us -> 74.3 us  [the longest x1 71.3 us: shards(): pl.pallas_call(kernel, out_shape=(out, out, square), in_specs=[hbm] * 13,...]
where the time goes in v2:
time: 75.1 us; the launch traced here: 75 us
  Pallas kernels  74.3 us (99%)
    pallas_call x1, Pallas kernels, shards(): pl.pallas_call(kernel, out_shape=(out, out, square), in_specs=[hbm] * 13,...  71.3 us
    pallas_call x1, Pallas kernels, shards(): pl.pallas_call(finish, out_shape=(out, out), in_specs=[hbm] * 3, out_spec...  3.01 us

profile of v2, /device:TPU:1, one launch (start us, length us, event | category | flops | bytes accessed | tf_op | source)
XLA Modules:
  0.0 75.0 jit_solution(10862768721213913040)
XLA Ops:
  0.6 71.3 %shard_map.140 = (bf16[256,2048]{1,0:T(8,128)(2,1)}, bf16[256,2048]{1,0:T(8,128)(2,1)}, bf16[256,256]{1,0:T(8,128)(2,1)}) custom-call(f32[3,128]{1,0:T(4,128)} %taps_hbm.1, f32[1,128]{1,0:T(1,128)} %bitcast.7, f32[1,2048]{1,0:T(1,128)} %bitcast.4, s32[2,256]{1,0:T(2,128)} %bitcast.5, f32[2,256]{1,0:T(2,128)} %bitcast.6, bf16[2048,128]{1,0:T(8,128)(2,1)} %og_hbm.1, ...), custom_call_target="tpu_custom_call" | custom-call | tf_op jit(solution)/shard_map/pallas_call | solution.py:455
  71.9 3.0 %shard_map.141 = (bf16[256,2048]{1,0:T(8,128)(2,1)}, bf16[256,2048]{1,0:T(8,128)(2,1)}) custom-call(bf16[256,256]{1,0:T(8,128)(2,1)} %get-tuple-element.5.perm_hbm, bf16[256,2048]{1,0:T(8,128)(2,1)} %get-tuple-element.6.ret_hbm, bf16[256,2048]{1,0:T(8,128)(2,1)} %get-tuple-element.7.mixed_hbm), custom_call_target="tpu_custom_call" | custom-call | tf_op jit(solution)/shard_map/pallas_call | solution.py:508

commit v3 on v2

v3 whole, which is shorter than its diff:
```python
import functools

import jax
import jax.numpy as jnp
from jax import lax
from jax.experimental import pallas as pl
from jax.experimental.pallas import tpu as pltpu
from jax.sharding import PartitionSpec as P

MESH = pl.DeviceIdType.MESH
F32 = jnp.float32
BF16 = jnp.bfloat16
EPS = 1e-06

SIDE = 4
ORDER = (
    ((1, 2), (2, 1), (0, 2), (2, 0)),
    ((2, 2), (2, 3), (3, 2), (1, 1)),
    ((3, 0), (1, 3), (3, 1), (3, 3)),
    ((0, 0), (0, 1), (1, 0), (0, 3)),
)
OFFSETS = tuple(pair for chunk in ORDER for pair in chunk)
CHUNKS = len(ORDER)
SELF = OFFSETS.index((0, 0))
SPLIT_ORDER = (3, 0, 1, 2)
PER_CHUNK = len(ORDER[0])
EP = len(OFFSETS)
TP = 8
GROUP_ROWS = 16
EXPERT_ROWS = 4
META = 128
GROUP_CH = 64
TP_ORDER = (4, 5, 2, 3, 6, 7, 1)
MIX_GROUPS = ((4, 5), (2, 3, 1), (6, 7))
NEAR = CHUNKS - 1
EDGE = 16


def chunk_peers(j):
    return [k for k in range(j * PER_CHUNK, (j + 1) * PER_CHUNK) if k != SELF]


def iota(shape, dim):
    return lax.broadcasted_iota(jnp.int32, shape, dim)


def hot(mask):
    return jnp.where(mask, 1.0, 0.0)


def dot(a, b, contract=((1,), (0,))):
    return lax.dot_general(a, b, (contract, ((), ())), preferred_element_type=F32)


def kernel(
    taps_hbm, ggain_hbm, mgain_hbm, ids_hbm, rw_hbm, og_hbm, ig_hbm, ci_hbm, mixw_hbm, x_hbm, wg_hbm, wu_hbm, wd_hbm,
    mixed, ret, perm,
    taps_ref, ggain_ref, mgain_ref, ids_ref, rw_ref,
    x_buf, xn_buf, og, ig, ci, normed, recvm, mixw, wg, wu, wd,
    send1, recv1, send2, recv2, hid, send3, res, send4, mixed_sum,
    load_sem, sent_sem, r1, r2, r3, r4, rm, re,
):
    ep = lax.axis_index("ep")
    tp = lax.axis_index("tp")
    z, x = ep // SIDE, ep % SIDE
    y, c = tp // 2, tp % 2
    tokens, width = x_buf.shape
    length = og.shape[0]

    def ep_peer(dz, dx):
        return (((z + dz) % SIDE) * SIDE + (x + dx) % SIDE, tp)

    def tp_peer(q, back=False):
        dy, dc = q // 2, q % 2
        dy = SIDE - dy if back else dy
        return (ep, ((y + dy) % SIDE) * 2 + (c + dc) % 2)

    def load(i, src, dst):
        cp = pltpu.make_async_copy(src, dst, load_sem.at[i])
        cp.start()
        return cp

    ld_ids = load(8, ids_hbm, ids_ref)
    ld_rw = load(9, rw_hbm, rw_ref)
    inner = pl.ds(EDGE, length)
    ld_ig = load(1, ig_hbm, ig.at[inner])
    ld_ci = load(2, ci_hbm, ci.at[inner])
    ld_og = load(3, og_hbm, og)
    ld_taps = load(11, taps_hbm, taps_ref)
    ld_ggain = load(12, ggain_hbm, ggain_ref)
    ld_x = load(0, x_hbm, x_buf)
    ld_mgain = load(10, mgain_hbm, mgain_ref)

    barrier = pltpu.get_barrier_semaphore()
    for k in range(EP):
        if k == SELF:
            continue
        dz, dx = OFFSETS[k]
        pl.semaphore_signal(barrier, inc=1, device_id=ep_peer(dz, dx), device_id_type=MESH)
    for q in range(1, TP):
        pl.semaphore_signal(barrier, inc=1, device_id=tp_peer(q), device_id_type=MESH)

    ld_wg = load(4, wg_hbm.at[0], wg)
    ld_wu = load(5, wu_hbm.at[0], wu)
    ld_wd = load(6, wd_hbm.at[0], wd)
    ld_mw = load(7, mixw_hbm, mixw)

    def send(src, dst, ssem, rsem, device):
        pltpu.make_async_remote_copy(
            src_ref=src, dst_ref=dst, send_sem=ssem, recv_sem=rsem, device_id=device, device_id_type=MESH
        ).start()

    def arrived(ref, sem):
        pltpu.make_async_remote_copy(
            src_ref=ref, dst_ref=ref, send_sem=sem, recv_sem=sem, device_id=tp_peer(1), device_id_type=MESH
        ).wait_recv()

    def departed(ref, sem):
        pltpu.make_async_remote_copy(
            src_ref=ref, dst_ref=ref, send_sem=sem, recv_sem=sem, device_id=tp_peer(1), device_id_type=MESH
        ).wait_send()

    ld_ids.wait()
    ld_rw.wait()
    id0 = ids_ref[0:1, :]
    id1 = ids_ref[1:2, :]
    earlier = hot(iota((tokens, tokens), 0) < iota((tokens, tokens), 1)).astype(BF16)
    expert_of = iota((EP * TP, tokens), 0)
    hits0 = hot(expert_of == id0)
    hits1 = hot(expert_of == id1)
    before = dot((hits0 + hits1).astype(BF16), earlier)
    rank0 = jnp.sum(hits0 * before, axis=0, keepdims=True)
    rank1 = jnp.sum(hits1 * before, axis=0, keepdims=True)

    def base_slot(ids, rank):
        inner = ids & (TP - 1)
        dy = ((inner >> 1) - y) & (SIDE - 1)
        dc = ((inner & 1) + c) & 1
        return ((dy * 2 + dc) * GROUP_ROWS).astype(F32) + rank

    base0 = base_slot(id0, rank0)
    base1 = base_slot(id1, rank1)
    group = id0 >> 3
    place = (((group >> 2) - z) & 3) * SIDE + (((group & 3) - x) & 3)
    order = jnp.zeros_like(place)
    for k, (dz, dx) in enumerate(OFFSETS):
        order = jnp.where(place == dz * SIDE + dx, k, order)
    members = hot(iota((EP, tokens), 0) == order)
    group_rank = jnp.sum(members * dot(members.astype(BF16), earlier), axis=0, keepdims=True)
    slot = (order * GROUP_ROWS).astype(F32) + group_rank
    perm_f32 = hot(iota((tokens, tokens), 0).astype(F32) == slot)
    forward = perm_f32.astype(BF16)
    w_hi = rw_ref[...].astype(BF16).astype(F32)
    w_lo = rw_ref[...] - w_hi
    meta_rows = jnp.concatenate(
        [base0, base1, w_hi[0:1], w_lo[0:1], w_hi[1:2], w_lo[1:2], jnp.zeros((META - 6, tokens), F32)], axis=0
    )
    meta = dot(forward, meta_rows.astype(BF16), ((1,), (1,))).astype(BF16)
    mine = slice(SELF * GROUP_ROWS, (SELF + 1) * GROUP_ROWS)
    send1[:, 0:META] = meta
    recv1[mine, 0:META] = meta[mine]

    ld_ig.wait()
    ld_ci.wait()
    pl.semaphore_wait(barrier, EP - 1 + TP - 1)
    after = (lax.rem(ep + 1, EP), tp)
    for ref in (ig, ci):
        send(ref.at[pl.ds(length, EDGE)], ref.at[pl.ds(0, EDGE)], sent_sem.at[5], re.at[0], after)

    ld_og.wait()
    ld_taps.wait()
    ld_ggain.wait()
    same = hot((iota((META, META), 0) >> 6) == (iota((META, META), 1) >> 6))
    averager = (same * (1.0 / GROUP_CH)).astype(BF16)

    def convolve(i):
        rows = pl.ds(pl.multiple_of(i * tokens, tokens), tokens)
        wide = pl.ds(pl.multiple_of(i * tokens, EDGE), tokens + EDGE)
        block = ig[wide, :].astype(F32) * ci[wide, :].astype(F32)
        keep = jnp.where(ep * TP + i > 0, 1.0, 0.0)
        block = jnp.concatenate([block[0:EDGE] * keep, block[EDGE:]], axis=0)
        convolved = (
            taps_ref[0:1, :] * pltpu.roll(block, 2, 0)[EDGE:]
            + taps_ref[1:2, :] * pltpu.roll(block, 1, 0)[EDGE:]
            + taps_ref[2:3, :] * block[EDGE:]
        )
        gated = og[rows, :].astype(F32) * convolved
        square = gated * gated
        high = square.astype(BF16)
        low = (square - high.astype(F32)).astype(BF16)
        inv = lax.rsqrt(dot(high, averager) + dot(low, averager) + EPS)
        normed[rows, :] = (gated * inv * ggain_ref[...]).astype(BF16)

    def convolve_chip(chip):
        convolve(chip * 2)
        convolve(chip * 2 + 1)

    def send_mixer(group):
        for q in MIX_GROUPS[group]:
            peer = tp_peer(q)
            rows = pl.ds(pl.multiple_of(peer[1] * tokens, tokens), tokens)
            send(normed.at[rows], recvm.at[tp], sent_sem.at[4], rm.at[group], peer)

    @pl.when(y == 2)
    def _():
        arrived(ig.at[pl.ds(0, 2 * EDGE)], re.at[0])

    convolve_chip((y + 2) % SIDE)
    send_mixer(0)

    ld_x.wait()
    ld_mgain.wait()
    wide_in = x_buf[...].astype(F32)
    scale = lax.rsqrt(jnp.mean(wide_in * wide_in, axis=-1, keepdims=True) + EPS)
    tile = 512
    tiles = [slice(n * tile, (n + 1) * tile) for n in range(width // tile)]
    half = len(tiles) // 2
    near = slice(NEAR * PER_CHUNK * GROUP_ROWS, tokens)
    halves = (pl.ds(0, META + width // 2), pl.ds(META + width // 2, width // 2))

    def shifted(cols):
        return slice(cols.start + META, cols.stop + META)

    def send_first(j, cols, sem):
        for k in chunk_peers(j):
            rows = pl.ds(k * GROUP_ROWS, GROUP_ROWS)
            send(send1.at[rows, cols], recv1.at[rows, cols], sent_sem.at[0], sem, ep_peer(*OFFSETS[k]))

    for n, cols in enumerate(tiles):
        tile_in = (x_buf[:, cols].astype(F32) * scale * mgain_ref[:, cols]).astype(BF16)
        xn_buf[:, cols] = tile_in
        moved = dot(forward[near], tile_in).astype(BF16)
        send1[near, shifted(cols)] = moved
        recv1[mine, shifted(cols)] = moved[mine.start - near.start : mine.stop - near.start]
        if n == half - 1:
            send_first(NEAR, halves[0], r1.at[NEAR])
    send_first(NEAR, halves[1], r1.at[CHUNKS])
    far = slice(0, near.start)
    for cols in tiles:
        send1[far, shifted(cols)] = dot(forward[far], xn_buf[:, cols]).astype(BF16)
    row = pl.ds(0, META + width)
    send_first(0, row, r1.at[0])
    perm[...] = perm_f32.T.astype(BF16)

    @pl.when(y != 2)
    def _():
        arrived(ig.at[pl.ds(0, 2 * EDGE)], re.at[0])

    convolve_chip((y + 1) % SIDE)
    convolve_chip(y)
    send_mixer(1)
    recvm[tp] = normed[pl.ds(pl.multiple_of(tp * tokens, tokens), tokens), :]

    chunk_in = PER_CHUNK * GROUP_ROWS
    chunk_out = TP * GROUP_ROWS

    def places(j):
        info = recv1[j * chunk_in : (j + 1) * chunk_in, 0:META].astype(F32)
        shift = ((iota((chunk_in, chunk_out), 0) >> 4) * EXPERT_ROWS).astype(F32)
        lane = iota((chunk_in, chunk_out), 1).astype(F32)
        return info, info[:, 0:1] + shift == lane, info[:, 1:2] + shift == lane

    def send_second(j, cols):
        for q in TP_ORDER:
            rows = pl.ds(j * chunk_out + q * GROUP_ROWS, GROUP_ROWS)
            send(send2.at[rows, cols], recv2.at[rows, cols], sent_sem.at[1], r2.at[j], tp_peer(q))

    def split_tile(j, split, cols):
        base = j * chunk_out
        moved = dot(split, recv1[j * chunk_in : (j + 1) * chunk_in, shifted(cols)]).astype(BF16)
        send2[base : base + chunk_out, cols] = moved
        recv2[base : base + GROUP_ROWS, cols] = moved[0:GROUP_ROWS]

    def splitter(j):
        _, at0, at1 = places(j)
        return (hot(at0) + hot(at1)).T.astype(BF16)

    others = pl.ds((NEAR * PER_CHUNK + 1) * GROUP_ROWS, (PER_CHUNK - 1) * GROUP_ROWS)
    whole = pl.ds(0, width)
    out_halves = (pl.ds(0, width // 2), pl.ds(width // 2, width // 2))
    arrived(recv1.at[others, halves[0]], r1.at[NEAR])
    split = splitter(NEAR)
    for cols in tiles[:half]:
        split_tile(NEAR, split, cols)
    send_second(NEAR, out_halves[0])
    arrived(recv1.at[others, halves[1]], r1.at[CHUNKS])
    for cols in tiles[half:]:
        split_tile(NEAR, split, cols)
    send_second(NEAR, out_halves[1])
    send_first(1, row, r1.at[1])
    convolve_chip((y + 3) % SIDE)
    for j in range(NEAR):
        arrived(recv1.at[pl.ds(j * chunk_in, chunk_in)], r1.at[j])
        if j == 0:
            send_first(2, row, r1.at[2])
        split = splitter(j)
        for cols in tiles:
            split_tile(j, split, cols)
        send_second(j, whole)

    ld_wg.wait()
    ld_wu.wait()
    ld_wd.wait()
    hidden_units = wg.shape[1]
    hid_tile = 256

    def send_third(j, cols, sem):
        for q in TP_ORDER:
            rows = pl.ds(j * chunk_out + q * GROUP_ROWS, GROUP_ROWS)
            send(send3.at[rows, cols], res.at[rows, cols], sent_sem.at[2], sem, tp_peer(q, back=True))

    for j in range(CHUNKS):
        base = j * chunk_out
        arrived(recv2.at[pl.ds(base + GROUP_ROWS, chunk_out - GROUP_ROWS)], r2.at[j])

        @pl.loop(0, hidden_units // hid_tile)
        def _(n):
            cols = pl.ds(pl.multiple_of(n * hid_tile, hid_tile), hid_tile)
            inputs = recv2[base : base + chunk_out, :]
            gate = dot(inputs, wg[:, cols])
            up = dot(inputs, wu[:, cols])
            hid[:, cols] = (gate / (1.0 + jnp.exp(-gate)) * up).astype(BF16)

        def down(n):
            cols = pl.ds(pl.multiple_of(n * tile, tile), tile)
            result = dot(hid[...], wd[:, cols]).astype(BF16)
            send3[base : base + chunk_out, cols] = result
            res[base : base + GROUP_ROWS, cols] = result[0:GROUP_ROWS]

        if j < NEAR:
            pl.loop(0, len(tiles))(down)
            send_third(j, whole, r3.at[j])
        else:
            pl.loop(0, half)(down)
            send_third(j, out_halves[0], r3.at[NEAR])
            pl.loop(half, len(tiles))(down)
            send_third(j, out_halves[1], r3.at[CHUNKS])
    send_mixer(2)

    def chip_part(dy, cols):
        chip = (y + dy) % SIDE
        pair = jnp.concatenate([recvm[chip * 2], recvm[chip * 2 + 1]], axis=1)
        weights = mixw[pl.ds(pl.multiple_of(chip * (2 * META), 2 * META), 2 * META), cols]
        return dot(pair, weights)

    ld_mw.wait()
    for group in (0, 1):
        arrived(recvm.at[pl.ds(0, len(MIX_GROUPS[group]))], rm.at[group])

    @pl.loop(0, len(tiles))
    def _(n):
        cols = pl.ds(pl.multiple_of(n * tile, tile), tile)
        mixed_sum[:, cols] = chip_part(0, cols) + chip_part(2, cols) + chip_part(3, cols)

    def weights_of(j):
        info, at0, at1 = places(j)
        high = jnp.where(at0, info[:, 2:3], 0.0) + jnp.where(at1, info[:, 4:5], 0.0)
        low = jnp.where(at0, info[:, 3:4], 0.0) + jnp.where(at1, info[:, 5:6], 0.0)
        return high.astype(BF16), low.astype(BF16)

    def join_tile(j, high, low, cols):
        base = j * chunk_in
        results = res[j * chunk_out : (j + 1) * chunk_out, cols]
        joined = (dot(high, results) + dot(low, results)).astype(BF16)
        send4[base : base + chunk_in, cols] = joined
        if j == NEAR:
            ret[mine, cols] = joined[mine.start - near.start : mine.stop - near.start]

    def send_home(j, cols):
        for k in chunk_peers(j):
            dz, dx = OFFSETS[k]
            rows = pl.ds(k * GROUP_ROWS, GROUP_ROWS)
            peer = ep_peer(SIDE - dz, SIDE - dx)
            send(send4.at[rows, cols], ret.at[rows, cols], sent_sem.at[3], r4.at[0], peer)

    for j in range(NEAR):
        high, low = weights_of(j)
        base = j * chunk_out
        arrived(res.at[pl.ds(base + GROUP_ROWS, chunk_out - GROUP_ROWS)], r3.at[j])
        for cols in tiles:
            join_tile(j, high, low, cols)
        send_home(j, whole)
    high, low = weights_of(NEAR)
    rows = pl.ds(NEAR * chunk_out + GROUP_ROWS, chunk_out - GROUP_ROWS)
    arrived(res.at[rows, out_halves[0]], r3.at[NEAR])
    for cols in tiles[:half]:
        join_tile(NEAR, high, low, cols)
    send_home(NEAR, out_halves[0])
    arrived(res.at[rows, out_halves[1]], r3.at[CHUNKS])
    for cols in tiles[half:]:
        join_tile(NEAR, high, low, cols)
    send_home(NEAR, out_halves[1])

    arrived(recvm.at[pl.ds(0, len(MIX_GROUPS[2]))], rm.at[2])
    for cols in tiles:
        mixed[:, cols] = (mixed_sum[:, cols] + chip_part(1, cols)).astype(BF16)

    remote_rows = pl.ds(0, (EP - 1) * GROUP_ROWS)
    remote_slots = pl.ds(0, CHUNKS * (chunk_out - GROUP_ROWS))
    departed(send1.at[remote_rows], sent_sem.at[0])
    departed(send2.at[remote_slots], sent_sem.at[1])
    departed(send3.at[remote_slots], sent_sem.at[2])
    departed(recvm.at[pl.ds(0, TP - 1)], sent_sem.at[4])
    departed(ig.at[pl.ds(0, 2 * EDGE)], sent_sem.at[5])
    departed(send4.at[remote_rows], sent_sem.at[3])
    arrived(send4.at[remote_rows], r4.at[0])


def finish(perm, ret, mixed, out_mixed, out_moe, moe, sem):
    width = ret.shape[1]
    steps = sem.shape[0] - 1
    tile = width // steps
    mixed_out = pltpu.make_async_copy(mixed, out_mixed, sem.at[steps])
    mixed_out.start()
    outs = []
    for n in range(steps):
        cols = slice(n * tile, (n + 1) * tile)
        moe[:, cols] = dot(perm[...], ret[:, cols]).astype(BF16)
        outs.append(pltpu.make_async_copy(moe.at[:, cols], out_moe.at[:, cols], sem.at[n]))
        outs[-1].start()
    for cp in outs:
        cp.wait()
    mixed_out.wait()


def shards(
    out_gate, in_gate, conv_input, conv_taps, group_gain, mix_out_w, moe_in, moe_gain, route_ids, route_weight,
    gate_w, up_w, down_w,
):
    rows, channels = in_gate.shape
    tokens, width = moe_in.shape
    hidden = gate_w.shape[2]
    hbm = pl.BlockSpec(memory_space=pltpu.HBM)
    vmem = pl.BlockSpec(memory_space=pltpu.VMEM)
    dma = pltpu.SemaphoreType.DMA
    V = pltpu.VMEM
    out = jax.ShapeDtypeStruct((tokens, width), BF16)
    square = jax.ShapeDtypeStruct((tokens, tokens), BF16)
    slots = 2 * tokens
    mixed, returned, perm = pl.pallas_call(
        kernel,
        out_shape=(out, out, square),
        in_specs=[hbm] * 13,
        out_specs=(vmem, vmem, vmem),
        scratch_shapes=[
            V(conv_taps.shape, F32),
            V((1, channels), F32),
            V((1, width), F32),
            V((2, tokens), jnp.int32),
            V((2, tokens), F32),
            V((tokens, width), BF16),
            V((tokens, width), BF16),
            V((rows, channels), BF16),
            V((rows + EDGE, channels), BF16),
            V((rows + EDGE, channels), BF16),
            V((rows, channels), BF16),
            V((TP, tokens, channels), BF16),
            V(mix_out_w.shape, BF16),
            V((width, hidden), BF16),
            V((width, hidden), BF16),
            V((hidden, width), BF16),
            V((tokens, META + width), BF16),
            V((tokens, META + width), BF16),
            V((slots, width), BF16),
            V((slots, width), BF16),
            V((TP * GROUP_ROWS, hidden), BF16),
            V((slots, width), BF16),
            V((slots, width), BF16),
            V((tokens, width), BF16),
            V((tokens, width), F32),
            dma((13,)),
            dma((6,)),
            dma((CHUNKS + 1,)),
            dma((CHUNKS,)),
            dma((CHUNKS + 1,)),
            dma((1,)),
            dma((len(MIX_GROUPS),)),
            dma((1,)),
        ],
        compiler_params=pltpu.CompilerParams(
            collective_id=0, has_side_effects=True, vmem_limit_bytes=48 * 1024 * 1024
        ),
    )(*[
        pltpu.with_memory_space_constraint(array, pltpu.HBM)
        for array in (
            conv_taps, group_gain.reshape(1, -1), moe_gain.reshape(1, -1), route_ids.T, route_weight.T,
            out_gate, in_gate, conv_input, mix_out_w, moe_in, gate_w, up_w, down_w,
        )
    ])
    return pl.pallas_call(
        finish,
        out_shape=(out, out),
        in_specs=[vmem] * 3,
        out_specs=(hbm, hbm),
        scratch_shapes=[V((tokens, width), BF16), dma((5,))],
        compiler_params=pltpu.CompilerParams(vmem_limit_bytes=12 * 1024 * 1024),
    )(perm, returned, mixed)


def solution(mesh):
    both = ("ep", "tp")
    in_specs = (
        P("ep", "tp"), P("ep", "tp"), P("ep", "tp"), P(None, "tp"), P("tp"), P(),
        P(both, None), P(), P(both, None), P(both, None),
        P(both, None, None), P(both, None, None), P(both, None, None),
    )
    return jax.shard_map(
        shards, mesh=mesh, in_specs=in_specs, out_specs=(P(both, None), P(both, None)), check_vma=False
    )
```

time: 75.1 us -> 69.7 us (0.928)
  Pallas kernels: 74.3 us -> 68.9 us
    pallas_call x1, Pallas kernels: 71.3 us -> 67.6 us  [shards(): pl.pallas_call(kernel, out_shape=(out, out, square), in_specs=[hbm] * 13,...]
    pallas_call x1, Pallas kernels: 3.01 us -> 1.35 us  [shards(): pl.pallas_call(finish, out_shape=(out, out), in_specs=[vmem] * 3, out_spe...]
where the time goes in v3:
time: 69.7 us; the launch traced here: 69.6 us
  Pallas kernels  68.9 us (99%)
    pallas_call x1, Pallas kernels, shards(): pl.pallas_call(kernel, out_shape=(out, out, square), in_specs=[hbm] * 13,...  67.6 us

profile of v3, /device:TPU:1, one launch (start us, length us, event | category | flops | bytes accessed | tf_op | source)
XLA Modules:
  0.0 69.6 jit_solution(6629369993684834000)
XLA Ops:
  0.6 67.6 %shard_map.140 = (bf16[256,2048]{1,0:T(8,128)(2,1)S(1)}, bf16[256,2048]{1,0:T(8,128)(2,1)S(1)}, bf16[256,256]{1,0:T(8,128)(2,1)S(1)}) custom-call(f32[3,128]{1,0:T(4,128)} %taps_hbm.1, f32[1,128]{1,0:T(1,128)} %bitcast.7, f32[1,2048]{1,0:T(1,128)} %bitcast.4, s32[2,256]{1,0:T(2,128)} %bitcast.5, f32[2,256]{1,0:T(2,128)} %bitcast.6, ...), custom_call_target="tpu_custom_call" | custom-call | tf_op jit(solution)/shard_map/pallas_call | solution.py:440
  68.2 1.4 %shard_map.141 = (bf16[256,2048]{1,0:T(8,128)(2,1)}, bf16[256,2048]{1,0:T(8,128)(2,1)}) custom-call(bf16[256,256]{1,0:T(8,128)(2,1)S(1)} %get-tuple-element.5.perm, bf16[256,2048]{1,0:T(8,128)(2,1)S(1)} %get-tuple-element.6.ret, bf16[256,2048]{1,0:T(8,128)(2,1)S(1)} %get-tuple-element.7.mixed), custom_call_target="tpu_custom_call" | custom-call | tf_op jit(solution)/shard_map/pallas_call | solution.py:490

commit v4 on v3

--- a/solution.py
+++ b/solution.py
@@ -31,7 +31,7 @@
 META = 128
 GROUP_CH = 64
 TP_ORDER = (4, 5, 2, 3, 6, 7, 1)
-MIX_GROUPS = ((4, 5), (2, 3, 1), (6, 7))
+MIX_GROUPS = ((4, 5), (1,), (2, 3, 6, 7))
 NEAR = CHUNKS - 1
 EDGE = 16
 
@@ -99,11 +99,6 @@
         pl.semaphore_signal(barrier, inc=1, device_id=ep_peer(dz, dx), device_id_type=MESH)
     for q in range(1, TP):
         pl.semaphore_signal(barrier, inc=1, device_id=tp_peer(q), device_id_type=MESH)
-
-    ld_wg = load(4, wg_hbm.at[0], wg)
-    ld_wu = load(5, wu_hbm.at[0], wu)
-    ld_wd = load(6, wd_hbm.at[0], wd)
-    ld_mw = load(7, mixw_hbm, mixw)
 
     def send(src, dst, ssem, rsem, device):
         pltpu.make_async_remote_copy(
@@ -201,15 +196,17 @@
             rows = pl.ds(pl.multiple_of(peer[1] * tokens, tokens), tokens)
             send(normed.at[rows], recvm.at[tp], sent_sem.at[4], rm.at[group], peer)
 
-    @pl.when(y == 2)
+    @pl.when(y != 2)
     def _():
-        arrived(ig.at[pl.ds(0, 2 * EDGE)], re.at[0])
-
-    convolve_chip((y + 2) % SIDE)
-    send_mixer(0)
+        convolve_chip((y + 2) % SIDE)
+        send_mixer(0)
 
     ld_x.wait()
     ld_mgain.wait()
+    ld_wg = load(4, wg_hbm.at[0], wg)
+    ld_wu = load(5, wu_hbm.at[0], wu)
+    ld_wd = load(6, wd_hbm.at[0], wd)
+    ld_mw = load(7, mixw_hbm, mixw)
     wide_in = x_buf[...].astype(F32)
     scale = lax.rsqrt(jnp.mean(wide_in * wide_in, axis=-1, keepdims=True) + EPS)
     tile = 512
@@ -242,11 +239,13 @@
     send_first(0, row, r1.at[0])
     perm[...] = perm_f32.T.astype(BF16)
 
-    @pl.when(y != 2)
+    arrived(ig.at[pl.ds(0, 2 * EDGE)], re.at[0])
+
+    @pl.when(y == 2)
     def _():
-        arrived(ig.at[pl.ds(0, 2 * EDGE)], re.at[0])
-
-    convolve_chip((y + 1) % SIDE)
+        convolve_chip((y + 2) % SIDE)
+        send_mixer(0)
+
     convolve_chip(y)
     send_mixer(1)
     recvm[tp] = normed[pl.ds(pl.multiple_of(tp * tokens, tokens), tokens), :]
@@ -288,6 +287,7 @@
         split_tile(NEAR, split, cols)
     send_second(NEAR, out_halves[1])
     send_first(1, row, r1.at[1])
+    convolve_chip((y + 1) % SIDE)
     convolve_chip((y + 3) % SIDE)
     for j in range(NEAR):
         arrived(recv1.at[pl.ds(j * chunk_in, chunk_in)], r1.at[j])
@@ -335,7 +335,6 @@
             send_third(j, out_halves[0], r3.at[NEAR])
             pl.loop(half, len(tiles))(down)
             send_third(j, out_halves[1], r3.at[CHUNKS])
-    send_mixer(2)
 
     def chip_part(dy, cols):
         chip = (y + dy) % SIDE
@@ -350,7 +349,7 @@
     @pl.loop(0, len(tiles))
     def _(n):
         cols = pl.ds(pl.multiple_of(n * tile, tile), tile)
-        mixed_sum[:, cols] = chip_part(0, cols) + chip_part(2, cols) + chip_part(3, cols)
+        mixed_sum[:, cols] = chip_part(0, cols) + chip_part(2, cols)
 
     def weights_of(j):
         info, at0, at1 = places(j)
@@ -380,6 +379,7 @@
         for cols in tiles:
             join_tile(j, high, low, cols)
         send_home(j, whole)
+    send_mixer(2)
     high, low = weights_of(NEAR)
     rows = pl.ds(NEAR * chunk_out + GROUP_ROWS, chunk_out - GROUP_ROWS)
     arrived(res.at[rows, out_halves[0]], r3.at[NEAR])
@@ -393,7 +393,7 @@
 
     arrived(recvm.at[pl.ds(0, len(MIX_GROUPS[2]))], rm.at[2])
     for cols in tiles:
-        mixed[:, cols] = (mixed_sum[:, cols] + chip_part(1, cols)).astype(BF16)
+        mixed[:, cols] = (mixed_sum[:, cols] + chip_part(1, cols) + chip_part(3, cols)).astype(BF16)
 
     remote_rows = pl.ds(0, (EP - 1) * GROUP_ROWS)
     remote_slots = pl.ds(0, CHUNKS * (chunk_out - GROUP_ROWS))

time: 69.7 us -> 67.8 us (0.973)
  Pallas kernels: 68.9 us -> 67 us
    pallas_call x1, Pallas kernels: 67.6 us -> 65.7 us  [shards(): pl.pallas_call(kernel, out_shape=(out, out, square), in_specs=[hbm] * 13,...]
where the time goes in v4:
time: 67.8 us; the launch traced here: 67.7 us
  Pallas kernels  67 us (99%)
    pallas_call x1, Pallas kernels, shards(): pl.pallas_call(kernel, out_shape=(out, out, square), in_specs=[hbm] * 13,...  65.7 us

profile of v4, /device:TPU:1, one launch (start us, length us, event | category | flops | bytes accessed | tf_op | source)
XLA Modules:
  0.0 67.7 jit_solution(10260019218397903756)
XLA Ops:
  0.6 65.7 %shard_map.140 = (bf16[256,2048]{1,0:T(8,128)(2,1)S(1)}, bf16[256,2048]{1,0:T(8,128)(2,1)S(1)}, bf16[256,256]{1,0:T(8,128)(2,1)S(1)}) custom-call(f32[3,128]{1,0:T(4,128)} %taps_hbm.1, f32[1,128]{1,0:T(1,128)} %bitcast.7, f32[1,2048]{1,0:T(1,128)} %bitcast.4, s32[2,256]{1,0:T(2,128)} %bitcast.5, f32[2,256]{1,0:T(2,128)} %bitcast.6, ...), custom_call_target="tpu_custom_call" | custom-call | tf_op jit(solution)/shard_map/pallas_call | solution.py:440
  66.3 1.4 %shard_map.141 = (bf16[256,2048]{1,0:T(8,128)(2,1)}, bf16[256,2048]{1,0:T(8,128)(2,1)}) custom-call(bf16[256,256]{1,0:T(8,128)(2,1)S(1)} %get-tuple-element.5.perm, bf16[256,2048]{1,0:T(8,128)(2,1)S(1)} %get-tuple-element.6.ret, bf16[256,2048]{1,0:T(8,128)(2,1)S(1)} %get-tuple-element.7.mixed), custom_call_target="tpu_custom_call" | custom-call | tf_op jit(solution)/shard_map/pallas_call | solution.py:490
